TPU v7x, 32 devices: a whole 2x2x4 slice. The times are simulated.
32 devices in a mesh: grp: 2 (over y), ra: 4 (over z), cb: 4 (over x, core).
Axes of the slice: x: 2, y: 2, z: 4, core: 2. Of those that a mesh axis runs over, the one named last changes fastest.
Arguments:
- stream: bfloat16 [256, 4096], P('grp', 'ra'), parts along dimension 0, may hold values from -180 to 180
- w_gate: float32 [2, 4096, 11264], P(None, 'ra', 'cb'), may hold values from -0.09375 to 0.09375
- w_up: float32 [2, 4096, 11264], P(None, 'ra', 'cb'), may hold values from -0.09375 to 0.09375
- w_down: float32 [2, 11264, 4096], P(None, 'cb', 'ra'), may hold values from -0.0546875 to 0.0546875
- gate_scale: float32 [2, 11264], P(None, 'cb'), may hold values from 0.5 to 2
- up_scale: float32 [2, 11264], P(None, 'cb'), may hold values from 0.5 to 2
- down_scale: float32 [2, 4096], P(None, 'ra'), may hold values from 0.5 to 2
- pre_gain: float32 [2, 4096], P(None, 'ra'), may hold values from 0.1 to 1.9
- out_gain: float32 [4096], P('ra'), may hold values from 0.1 to 1.9
Outputs:
- normed: bfloat16 [256, 4096], P('grp', 'ra'), parts along dimension 0
There are 2 independent parts, one for each index of `grp`. A program takes and returns all parts, laid end to end along the dimension named above; an argument that names none is the same for every part. Nothing has to cross between parts.
All inputs are finite; a program needn't handle non-finite values.
Results may differ from a plain program's by a relative error of at most 0.018.
Values may be sent and summed in bfloat16 or wider, within the bound.
A program may use at most 192 MiB of HBM per device.

v0:
```python
import jax
import jax.numpy as jnp
from jax import lax
from jax.sharding import PartitionSpec as P

D = 4096
LAYERS = 2


def local(stream, w_gate, w_up, w_down, gate_scale, up_scale, down_scale, pre_gain, out_gain):
    current = stream
    tokens = stream.shape[0]
    share = tokens // lax.axis_size("ra")
    for layer in range(LAYERS):
        xvals = current.astype(jnp.float32)
        squares = jnp.sum(xvals * xvals, axis=1)
        scaled = (xvals * pre_gain[layer]).astype(jnp.bfloat16)
        gate_part = jnp.dot(
            scaled, w_gate[layer].astype(jnp.bfloat16), preferred_element_type=jnp.float32
        )
        up_part = jnp.dot(
            scaled, w_up[layer].astype(jnp.bfloat16), preferred_element_type=jnp.float32
        )
        down_local = w_down[layer].astype(jnp.bfloat16)
        total = lax.psum(squares, "ra")
        operands = (gate_part, up_part)
        summed = (
            lax.psum_scatter(operands[0], "ra", scatter_dimension=0, tiled=True),
            lax.psum_scatter(operands[1], "ra", scatter_dimension=0, tiled=True),
        )
        own_rows = lax.dynamic_slice_in_dim(total, lax.axis_index("ra") * share, share)
        rinv = lax.rsqrt(own_rows / D + 1e-06)[:, None]
        gate = summed[0] * rinv * gate_scale[layer]
        upper = summed[1] * rinv * up_scale[layer]
        hidden = (jax.nn.silu(gate) * upper).astype(jnp.bfloat16)
        terms = jnp.dot(
            lax.all_gather(hidden, "ra", axis=0, tiled=True),
            down_local,
            preferred_element_type=jnp.float32,
        )
        branch = lax.psum(terms.astype(jnp.bfloat16), "cb").astype(jnp.float32) * down_scale[layer]
        current = (0.5 * xvals + branch).astype(jnp.bfloat16)
    xvals = current.astype(jnp.float32)
    final_sum = lax.psum(jnp.sum(xvals * xvals, axis=1), "ra")
    rinv = lax.rsqrt(final_sum / D + 1e-06)[:, None]
    return (xvals * rinv * out_gain).astype(jnp.bfloat16)


def solution(mesh):
    placed = (
        P("grp", "ra"),
        P(None, "ra", "cb"),
        P(None, "ra", "cb"),
        P(None, "cb", "ra"),
        P(None, "cb"),
        P(None, "cb"),
        P(None, "ra"),
        P(None, "ra"),
        P("ra"),
    )
    return jax.shard_map(
        local, mesh=mesh, in_specs=placed, out_specs=P("grp", "ra"), check_vma=False
    )
```

profile of v0, /device:TPU:0, one launch (start us, length us, event | category | flops | bytes accessed | tf_op | source)
XLA Modules:
  0.0 296.9 jit_solution(10310652706290276706)
XLA Ops:
  7.3 8.6 %convert.12 = bf16[2,1024,2816]{2,1,0:T(8,128)(2,1)S(1)} convert(f32[2,1024,2816]{2,1,0:T(8,128)} %param.10) | non-fusion elementwise | flops 5767168 | bytes 34603008 | tf_op jit(solution)/shard_map/convert.5
  15.9 4.2 %copy-done.1 = bf16[2,1024,2816]{2,1,0:T(8,128)(2,1)} copy-done((bf16[2,1024,2816]{2,1,0:T(8,128)(2,1)}, bf16[2,1024,2816]{2,1,0:T(8,128)(2,1)S(1)}, u32[]{:S(2)}) %copy-start.1) | copy-done | bytes 11534360
  20.1 2.0 fusion.5
  22.2 8.6 %convert.13 = bf16[2,1024,2816]{2,1,0:T(8,128)(2,1)S(1)} convert(f32[2,1024,2816]{2,1,0:T(8,128)} %param.11) | non-fusion elementwise | flops 5767168 | bytes 34603008 | tf_op jit(solution)/shard_map/convert.4
  30.8 4.2 %copy-done = bf16[2,1024,2816]{2,1,0:T(8,128)(2,1)} copy-done((bf16[2,1024,2816]{2,1,0:T(8,128)(2,1)}, bf16[2,1024,2816]{2,1,0:T(8,128)(2,1)S(1)}, u32[]{:S(2)}) %copy-start) | copy-done | bytes 11534360
  35.0 2.1 fusion.4
  37.2 12.6 %convert.14 = bf16[2,2816,1024]{2,1,0:T(8,128)(2,1)} convert(f32[2,2816,1024]{2,1,0:T(8,128)} %param.12) | non-fusion elementwise | flops 5767168 | bytes 34603008 | tf_op jit(solution)/shard_map/convert.3
  50.0 13.6 %psum.35 = f32[128]{0:T(128)S(1)} all-reduce(f32[128]{0:T(128)S(1)} %fusion.14), channel_id=1, replica_groups=mesh['grp'=2,'ra'=4,'cb'=4] {'ra'}, use_global_device_ids=true, to_apply=%region_2.0 | all-reduce | flops 128 | bytes 1024 | tf_op jit(solution)/shard_map/psum | solution.py:25
  63.8 29.2 %reduce-scatter.7.cloned.1.call-done = f32[32,2816]{1,0:T(8,128)} async-done(((f32[128,2816]{1,0:T(8,128)}), f32[32,2816]{1,0:T(8,128)}) %reduce-scatter.7.cloned.1.call-update) | async-done | bytes 360464 | tf_op jit(solution)/shard_map/reduce_scatter | solution.py:29
  93.0 1.3 multiply_convert_fusion.1
  94.3 17.2 %all_gather.6 = bf16[128,2816]{1,0:T(8,128)(2,1)S(1)} all-gather(bf16[32,2816]{1,0:T(8,128)(2,1)S(1)} %multiply_convert_fusion.1), channel_id=1, replica_groups=mesh['grp'=2,'ra'=4,'cb'=4] {'ra'}, dimensions={0}, use_global_device_ids=true | all-gather | bytes 901120 | tf_op jit(solution)/shard_map/all_gather | solution.py:37
  111.5 4.3 %fusion.6 = bf16[128,1024]{1,0:T(8,128)(2,1)} fusion(bf16[128,2816]{1,0:T(8,128)(2,1)S(1)} %all_gather.6, bf16[2,2816,1024]{2,1,0:T(8,128)(2,1)} %convert.14), kind=kOutput, calls=%fused_computation.12 | convolution fusion | flops 738328576 | bytes 6750208 | tf_op jit(solution)/shard_map/dot_general | solution.py:36
  115.9 31.3 %all-reduce.3.cloned.1.call-done = bf16[128,1024]{1,0:T(8,128)(2,1)} async-done(((bf16[128,1024]{1,0:T(8,128)(2,1)}), bf16[128,1024]{1,0:T(8,128)(2,1)}) %all-reduce.3.cloned.1.call-update) | async-done | bytes 262160 | tf_op jit(solution)/shard_map/psum | solution.py:41
  148.4 4.7 %fusion.2 = f32[128,2816]{1,0:T(8,128)} fusion(bf16[2,1024,2816]{2,1,0:T(8,128)(2,1)} %copy-done.1, bf16[128,1024]{1,0:T(8,128)(2,1)S(1)} %get-tuple-element.10, f32[1024]{0:T(1024)S(1)} %bitcast.31), kind=kOutput, calls=%fused_computation.5 | convolution fusion | flops 738590720 | bytes 7475200 | tf_op jit(solution)/shard_map/dot_general | solution.py:18
  153.1 4.7 %fusion.1 = f32[128,2816]{1,0:T(8,128)} fusion(bf16[2,1024,2816]{2,1,0:T(8,128)(2,1)} %copy-done, bf16[128,1024]{1,0:T(8,128)(2,1)S(1)} %get-tuple-element.10, f32[1024]{0:T(1024)S(1)} %bitcast.32), kind=kOutput, calls=%fused_computation.3 | convolution fusion | flops 738590720 | bytes 7475200 | tf_op jit(solution)/shard_map/dot_general | solution.py:21
  157.9 12.3 %psum.37 = f32[128]{0:T(128)S(1)} all-reduce(f32[128]{0:T(128)S(1)} %get-tuple-element.9), channel_id=1, replica_groups=mesh['grp'=2,'ra'=4,'cb'=4] {'ra'}, use_global_device_ids=true, to_apply=%region_7.8 | all-reduce | flops 128 | bytes 1024 | tf_op jit(solution)/shard_map/psum | solution.py:25
  170.3 16.5 %reduce-scatter.9.cloned.1.call-done = f32[32,2816]{1,0:T(8,128)} async-done(((f32[128,2816]{1,0:T(8,128)}), f32[32,2816]{1,0:T(8,128)}) %reduce-scatter.9.cloned.1.call-update) | async-done | bytes 360464 | tf_op jit(solution)/shard_map/reduce_scatter | solution.py:28
  186.8 34.4 %reduce-scatter.11.cloned.1.call-done = f32[32,2816]{1,0:T(8,128)} async-done(((f32[128,2816]{1,0:T(8,128)}), f32[32,2816]{1,0:T(8,128)}) %reduce-scatter.11.cloned.1.call-update) | async-done | bytes 360464 | tf_op jit(solution)/shard_map/reduce_scatter | solution.py:29
  221.2 1.3 multiply_convert_fusion
  222.5 17.2 %all_gather.7 = bf16[128,2816]{1,0:T(8,128)(2,1)S(1)} all-gather(bf16[32,2816]{1,0:T(8,128)(2,1)S(1)} %multiply_convert_fusion), channel_id=1, replica_groups=mesh['grp'=2,'ra'=4,'cb'=4] {'ra'}, dimensions={0}, use_global_device_ids=true | all-gather | bytes 901120 | tf_op jit(solution)/shard_map/all_gather | solution.py:37
  239.6 4.3 %fusion.7 = bf16[128,1024]{1,0:T(8,128)(2,1)} fusion(bf16[128,2816]{1,0:T(8,128)(2,1)S(1)} %all_gather.7, bf16[2,2816,1024]{2,1,0:T(8,128)(2,1)} %convert.14), kind=kOutput, calls=%fused_computation.13 | convolution fusion | flops 738328576 | bytes 6750208 | tf_op jit(solution)/shard_map/dot_general | solution.py:36
  244.0 31.5 %all-reduce.5.cloned.1.call-done = bf16[128,1024]{1,0:T(8,128)(2,1)} async-done(((bf16[128,1024]{1,0:T(8,128)(2,1)}), bf16[128,1024]{1,0:T(8,128)(2,1)}) %all-reduce.5.cloned.1.call-update) | async-done | bytes 262160 | tf_op jit(solution)/shard_map/psum | solution.py:41
  276.6 11.7 %psum.39 = f32[128]{0:T(128)S(1)} all-reduce(f32[128]{0:T(128)S(1)} %fusion.8), channel_id=1, replica_groups=mesh['grp'=2,'ra'=4,'cb'=4] {'ra'}, use_global_device_ids=true, to_apply=%region_11.12 | all-reduce | flops 128 | bytes 1024 | tf_op jit(solution)/shard_map/psum | solution.py:44
  288.3 1.8 fusion.10
  (34 shorter events, 3.9 us)
Async XLA Ops:
  6.5 57.3 %reduce-scatter.5.cloned.1.call-start = ((), (), s32[]{:S(2)}) async-start(), calls=%async_computation.4 | async-start | bytes 1802240 | tf_op jit(solution)/shard_map/reduce_scatter | solution.py:28
  7.3 12.8 %copy-start.2 = (bf16[128,1024]{1,0:T(8,128)(2,1)S(1)}, bf16[128,1024]{1,0:T(8,128)(2,1)}, u32[]{:S(2)}) copy-start(bf16[128,1024]{1,0:T(8,128)(2,1)} %param.9) | copy-start | bytes 786436
  15.9 4.2 %copy-start.1 = (bf16[2,1024,2816]{2,1,0:T(8,128)(2,1)}, bf16[2,1024,2816]{2,1,0:T(8,128)(2,1)S(1)}, u32[]{:S(2)}) copy-start(bf16[2,1024,2816]{2,1,0:T(8,128)(2,1)S(1)} %convert.12) | copy-start | bytes 34603012
  22.2 70.9 %reduce-scatter.7.cloned.1.call-start = ((), (), s32[]{:S(2)}) async-start(), calls=%async_computation.5 | async-start | bytes 1802240 | tf_op jit(solution)/shard_map/reduce_scatter | solution.py:29
  30.8 4.2 %copy-start = (bf16[2,1024,2816]{2,1,0:T(8,128)(2,1)}, bf16[2,1024,2816]{2,1,0:T(8,128)(2,1)S(1)}, u32[]{:S(2)}) copy-start(bf16[2,1024,2816]{2,1,0:T(8,128)(2,1)S(1)} %convert.13) | copy-start | bytes 34603012
  37.1 110.1 %all-reduce.3.cloned.1.call-start = ((), (), s32[]{:S(2)}) async-start(), calls=%async_computation.6 | async-start | bytes 524288 | tf_op jit(solution)/shard_map/psum | solution.py:41
  37.2 26.5 %copy-start.3 = (f32[2,2816]{1,0:T(2,128)S(1)}, f32[2,2816]{1,0:T(2,128)}, u32[]{:S(2)}) copy-start(f32[2,2816]{1,0:T(2,128)} %param.14) | copy-start | bytes 67588
  37.2 26.5 %copy-start.4 = (f32[2,2816]{1,0:T(2,128)S(1)}, f32[2,2816]{1,0:T(2,128)}, u32[]{:S(2)}) copy-start(f32[2,2816]{1,0:T(2,128)} %param.13) | copy-start | bytes 67588
  49.8 66.1 %copy-start.5 = (f32[2,1024]{1,0:T(2,128)S(1)}, f32[2,1024]{1,0:T(2,128)}, u32[]{:S(2)}) copy-start(f32[2,1024]{1,0:T(2,128)} %param.15) | copy-start | bytes 24580
  115.8 71.0 %reduce-scatter.9.cloned.1.call-start = ((), (), s32[]{:S(2)}) async-start(), calls=%async_computation.7 | async-start | bytes 1802240 | tf_op jit(solution)/shard_map/reduce_scatter | solution.py:28
  153.1 68.1 %reduce-scatter.11.cloned.1.call-start = ((), (), s32[]{:S(2)}) async-start(), calls=%async_computation.8 | async-start | bytes 1802240 | tf_op jit(solution)/shard_map/reduce_scatter | solution.py:29
  157.8 130.5 %copy-start.6 = (f32[1024]{0:T(1024)S(1)}, f32[1024]{0:T(1024)}, u32[]{:S(2)}) copy-start(f32[1024]{0:T(1024)} %param.17) | copy-start | bytes 12292
  157.9 117.6 %all-reduce.5.cloned.1.call-start = ((), (), s32[]{:S(2)}) async-start(), calls=%async_computation.9 | async-start | bytes 524288 | tf_op jit(solution)/shard_map/psum | solution.py:41
Sparse Core Ops, SparseCore 0:
  22.3 36.0 reduce-scatter.4
  60.8 32.2 reduce-scatter.6
  116.0 31.2 all-reduce.2
  153.2 33.5 reduce-scatter.8
  189.0 32.1 reduce-scatter.10
  244.1 31.3 all-reduce.4
where the time goes:
time: 298 us; the launch traced here: 297 us
  waiting for transfers between devices  143 us (48%)
  blocking collectives  71.9 us (24%)
  other arithmetic  36.8 us (12%)
  matrix products  22 us (7%)
  between operations  13.6 us (5%)
  local copies, waits for them, and re-layouts  9.34 us (3%)
    reduce_scatter x2, waiting for transfers between devices, local(): lax.psum_scatter(operands[1], 'ra', scatter_dimension=0, tiled=True)  63.6 us
    psum x2, waiting for transfers between devices, local(): lax.psum(terms.astype(jnp.bfloat16), 'cb').astype(jnp.float32)  62.8 us
    all_gather x2, blocking collectives, local(): lax.all_gather(hidden, 'ra', axis=0, tiled=True)  34.3 us
    another operation x3, other arithmetic  29.8 us
    psum x2, blocking collectives, local(): total = lax.psum(squares, 'ra')  25.9 us
    reduce_scatter x2, waiting for transfers between devices, local(): lax.psum_scatter(operands[0], 'ra', scatter_dimension=0, tiled=True)  16.6 us
    psum x1, blocking collectives, local(): final_sum = lax.psum(jnp.sum(xvals * xvals, axis=1), 'ra')  11.7 us
    dot_general x2, matrix products, local(): jnp.dot(lax.all_gather(hidden, 'ra', axis=0, tiled=True), down_local, pre...  8.61 us
  transfers between devices with their start and end apart: 6, of which 5 were waited for; matrix products, arithmetic and copies ran while one was open for 10% of the time, Pallas kernels for 0%

commit v1 on v0

--- a/solution.py
+++ b/solution.py
@@ -22,7 +22,9 @@
             scaled, w_up[layer].astype(jnp.bfloat16), preferred_element_type=jnp.float32
         )
         down_local = w_down[layer].astype(jnp.bfloat16)
-        total = lax.psum(squares, "ra")
+        total = squares
+        for hop in (1, 2):
+            total = total + lax.ppermute(total, "ra", [(dev, dev ^ hop) for dev in range(4)])
         operands = (gate_part, up_part)
         summed = (
             lax.psum_scatter(operands[0], "ra", scatter_dimension=0, tiled=True),

time: 298 us -> 297 us (level)
  blocking collectives: 71.9 us -> 46 us
  waiting for transfers between devices: 143 us -> 158 us
  starting transfers between devices: 0.21 us -> 10.5 us
    psum x2 -> x0, blocking collectives: 25.9 us -> none  [local(): total = lax.psum(squares, 'ra')]
    ppermute x0 -> x4, starting transfers between devices: none -> 10.3 us  [local(): lax.ppermute(total, 'ra', [(dev, dev ^ hop) for dev in range(4)])]
    ppermute x0 -> x4, waiting for transfers between devices: none -> 6.06 us  [local(): lax.ppermute(total, 'ra', [(dev, dev ^ hop) for dev in range(4)])]
    reduce_scatter x2, waiting for transfers between devices: 63.6 us -> 68.8 us  [local(): lax.psum_scatter(operands[1], 'ra', scatter_dimension=0, tiled=True)]
    reduce_scatter x2, waiting for transfers between devices: 16.6 us -> 20.7 us  [local(): lax.psum_scatter(operands[0], 'ra', scatter_dimension=0, tiled=True)]
  transfers between devices with their start and end apart: 6 -> 10, of which waited for: 5 -> 9; matrix products, arithmetic and copies ran while one was open for 10% -> 10% of each run, Pallas kernels for 0% -> 0%
where the time goes in v1:
time: 297 us
  waiting for transfers between devices  158 us (53%)
  blocking collectives  46 us (15%)
  other arithmetic  36.8 us (12%)
  matrix products  22 us (7%)
  between operations  13.6 us (5%)
  starting transfers between devices  10.5 us (4%)
  local copies, waits for them, and re-layouts  9.33 us (3%)
    reduce_scatter x2, waiting for transfers between devices, local(): lax.psum_scatter(operands[1], 'ra', scatter_dimension=0, tiled=True)  68.8 us
    psum x2, waiting for transfers between devices, local(): lax.psum(terms.astype(jnp.bfloat16), 'cb').astype(jnp.float32)  62.8 us
    all_gather x2, blocking collectives, local(): lax.all_gather(hidden, 'ra', axis=0, tiled=True)  34.3 us
    another operation x3, other arithmetic  29.8 us
    reduce_scatter x2, waiting for transfers between devices, local(): lax.psum_scatter(operands[0], 'ra', scatter_dimension=0, tiled=True)  20.7 us
    psum x1, blocking collectives, local(): final_sum = lax.psum(jnp.sum(xvals * xvals, axis=1), 'ra')  11.7 us
    ppermute x4, starting transfers between devices, local(): lax.ppermute(total, 'ra', [(dev, dev ^ hop) for dev in range(4)])  10.3 us
    dot_general x2, matrix products, local(): jnp.dot(lax.all_gather(hidden, 'ra', axis=0, tiled=True), down_local, pre...  8.61 us
  transfers between devices with their start and end apart: 10, of which 9 were waited for; matrix products, arithmetic and copies ran while one was open for 10% of the time, Pallas kernels for 0%

profile of v1, /device:TPU:0, one launch (start us, length us, event | category | flops | bytes accessed | tf_op | source)
XLA Modules:
  0.0 296.7 jit_solution(12217988240336290537)
XLA Ops:
  7.3 8.6 %convert.12 = bf16[2,1024,2816]{2,1,0:T(8,128)(2,1)S(1)} convert(f32[2,1024,2816]{2,1,0:T(8,128)} %param.10) | non-fusion elementwise | flops 5767168 | bytes 34603008 | tf_op jit(solution)/shard_map/convert.5
  15.9 4.2 %copy-done.1 = bf16[2,1024,2816]{2,1,0:T(8,128)(2,1)} copy-done((bf16[2,1024,2816]{2,1,0:T(8,128)(2,1)}, bf16[2,1024,2816]{2,1,0:T(8,128)(2,1)S(1)}, u32[]{:S(2)}) %copy-start.1) | copy-done | bytes 11534360
  20.1 2.0 fusion.5
  22.2 8.6 %convert.13 = bf16[2,1024,2816]{2,1,0:T(8,128)(2,1)S(1)} convert(f32[2,1024,2816]{2,1,0:T(8,128)} %param.11) | non-fusion elementwise | flops 5767168 | bytes 34603008 | tf_op jit(solution)/shard_map/convert.4
  30.8 4.2 %copy-done = bf16[2,1024,2816]{2,1,0:T(8,128)(2,1)} copy-done((bf16[2,1024,2816]{2,1,0:T(8,128)(2,1)}, bf16[2,1024,2816]{2,1,0:T(8,128)(2,1)S(1)}, u32[]{:S(2)}) %copy-start) | copy-done | bytes 11534360
  35.0 2.1 fusion.4
  37.3 3.3 %collective-permute-start = (f32[128]{0:T(128)S(1)}, f32[128]{0:T(128)S(1)}, u32[]{:S(2)}, u32[]{:S(2)}) collective-permute-start(f32[128]{0:T(128)S(1)} %fusion.14), channel_id=1, source_target_pairs={{0,4},{4,0},{8,12},{12,8},{1,5},{5,1},{9,13},{13,9},{2,6},{6,2},{1... | collective-permute-start | bytes 1544 | tf_op jit(solution)/shard_map/ppermute | solution.py:27
  42.4 3.0 collective-permute-start.1
  45.4 12.6 %convert.14 = bf16[2,2816,1024]{2,1,0:T(8,128)(2,1)} convert(f32[2,2816,1024]{2,1,0:T(8,128)} %param.12) | non-fusion elementwise | flops 5767168 | bytes 34603008 | tf_op jit(solution)/shard_map/convert.3
  58.5 34.5 %reduce-scatter.7.cloned.1.call-done = f32[32,2816]{1,0:T(8,128)} async-done(((f32[128,2816]{1,0:T(8,128)}), f32[32,2816]{1,0:T(8,128)}) %reduce-scatter.7.cloned.1.call-update) | async-done | bytes 360464 | tf_op jit(solution)/shard_map/reduce_scatter | solution.py:31
  94.3 17.2 %all_gather.6 = bf16[128,2816]{1,0:T(8,128)(2,1)S(1)} all-gather(bf16[32,2816]{1,0:T(8,128)(2,1)S(1)} %multiply_convert_fusion.1), channel_id=1, replica_groups=mesh['grp'=2,'ra'=4,'cb'=4] {'ra'}, dimensions={0}, use_global_device_ids=true | all-gather | bytes 901120 | tf_op jit(solution)/shard_map/all_gather | solution.py:39
  111.4 4.3 %fusion.6 = bf16[128,1024]{1,0:T(8,128)(2,1)} fusion(bf16[128,2816]{1,0:T(8,128)(2,1)S(1)} %all_gather.6, bf16[2,2816,1024]{2,1,0:T(8,128)(2,1)} %convert.14), kind=kOutput, calls=%fused_computation.12 | convolution fusion | flops 738328576 | bytes 6750208 | tf_op jit(solution)/shard_map/dot_general | solution.py:38
  115.9 31.3 %all-reduce.3.cloned.1.call-done = bf16[128,1024]{1,0:T(8,128)(2,1)} async-done(((bf16[128,1024]{1,0:T(8,128)(2,1)}), bf16[128,1024]{1,0:T(8,128)(2,1)}) %all-reduce.3.cloned.1.call-update) | async-done | bytes 262160 | tf_op jit(solution)/shard_map/psum | solution.py:43
  148.3 4.7 %fusion.2 = f32[128,2816]{1,0:T(8,128)} fusion(bf16[2,1024,2816]{2,1,0:T(8,128)(2,1)} %copy-done.1, bf16[128,1024]{1,0:T(8,128)(2,1)S(1)} %get-tuple-element.10, f32[1024]{0:T(1024)S(1)} %bitcast.31), kind=kOutput, calls=%fused_computation.5 | convolution fusion | flops 738590720 | bytes 7475200 | tf_op jit(solution)/shard_map/dot_general | solution.py:18
  153.1 4.7 %fusion.1 = f32[128,2816]{1,0:T(8,128)} fusion(bf16[2,1024,2816]{2,1,0:T(8,128)(2,1)} %copy-done, bf16[128,1024]{1,0:T(8,128)(2,1)S(1)} %get-tuple-element.10, f32[1024]{0:T(1024)S(1)} %bitcast.32), kind=kOutput, calls=%fused_computation.3 | convolution fusion | flops 738590720 | bytes 7475200 | tf_op jit(solution)/shard_map/dot_general | solution.py:21
  159.4 2.1 collective-permute-done.2
  161.5 2.4 collective-permute-start.3
  163.9 2.3 collective-permute-done.3
  166.3 20.3 %reduce-scatter.9.cloned.1.call-done = f32[32,2816]{1,0:T(8,128)} async-done(((f32[128,2816]{1,0:T(8,128)}), f32[32,2816]{1,0:T(8,128)}) %reduce-scatter.9.cloned.1.call-update) | async-done | bytes 360464 | tf_op jit(solution)/shard_map/reduce_scatter | solution.py:30
  186.6 34.3 %reduce-scatter.11.cloned.1.call-done = f32[32,2816]{1,0:T(8,128)} async-done(((f32[128,2816]{1,0:T(8,128)}), f32[32,2816]{1,0:T(8,128)}) %reduce-scatter.11.cloned.1.call-update) | async-done | bytes 360464 | tf_op jit(solution)/shard_map/reduce_scatter | solution.py:31
  222.2 17.1 %all_gather.7 = bf16[128,2816]{1,0:T(8,128)(2,1)S(1)} all-gather(bf16[32,2816]{1,0:T(8,128)(2,1)S(1)} %multiply_convert_fusion), channel_id=1, replica_groups=mesh['grp'=2,'ra'=4,'cb'=4] {'ra'}, dimensions={0}, use_global_device_ids=true | all-gather | bytes 901120 | tf_op jit(solution)/shard_map/all_gather | solution.py:39
  239.4 4.3 %fusion.7 = bf16[128,1024]{1,0:T(8,128)(2,1)} fusion(bf16[128,2816]{1,0:T(8,128)(2,1)S(1)} %all_gather.7, bf16[2,2816,1024]{2,1,0:T(8,128)(2,1)} %convert.14), kind=kOutput, calls=%fused_computation.13 | convolution fusion | flops 738328576 | bytes 6750208 | tf_op jit(solution)/shard_map/dot_general | solution.py:38
  243.7 31.5 %all-reduce.5.cloned.1.call-done = bf16[128,1024]{1,0:T(8,128)(2,1)} async-done(((bf16[128,1024]{1,0:T(8,128)(2,1)}), bf16[128,1024]{1,0:T(8,128)(2,1)}) %all-reduce.5.cloned.1.call-update) | async-done | bytes 262160 | tf_op jit(solution)/shard_map/psum | solution.py:43
  276.3 11.7 %psum.23 = f32[128]{0:T(128)S(1)} all-reduce(f32[128]{0:T(128)S(1)} %fusion.8), channel_id=1, replica_groups=mesh['grp'=2,'ra'=4,'cb'=4] {'ra'}, use_global_device_ids=true, to_apply=%region_9.10 | all-reduce | flops 128 | bytes 1024 | tf_op jit(solution)/shard_map/psum | solution.py:46
  (44 shorter events, 11.8 us)
Async XLA Ops:
  6.5 51.9 %reduce-scatter.5.cloned.1.call-start = ((), (), s32[]{:S(2)}) async-start(), calls=%async_computation.4 | async-start | bytes 1802240 | tf_op jit(solution)/shard_map/reduce_scatter | solution.py:30
  7.3 12.8 %copy-start.2 = (bf16[128,1024]{1,0:T(8,128)(2,1)S(1)}, bf16[128,1024]{1,0:T(8,128)(2,1)}, u32[]{:S(2)}) copy-start(bf16[128,1024]{1,0:T(8,128)(2,1)} %param.9) | copy-start | bytes 786436
  15.9 4.2 %copy-start.1 = (bf16[2,1024,2816]{2,1,0:T(8,128)(2,1)}, bf16[2,1024,2816]{2,1,0:T(8,128)(2,1)S(1)}, u32[]{:S(2)}) copy-start(bf16[2,1024,2816]{2,1,0:T(8,128)(2,1)S(1)} %convert.12) | copy-start | bytes 34603012
  22.2 70.8 %reduce-scatter.7.cloned.1.call-start = ((), (), s32[]{:S(2)}) async-start(), calls=%async_computation.5 | async-start | bytes 1802240 | tf_op jit(solution)/shard_map/reduce_scatter | solution.py:31
  30.8 4.2 %copy-start = (bf16[2,1024,2816]{2,1,0:T(8,128)(2,1)}, bf16[2,1024,2816]{2,1,0:T(8,128)(2,1)S(1)}, u32[]{:S(2)}) copy-start(bf16[2,1024,2816]{2,1,0:T(8,128)(2,1)S(1)} %convert.13) | copy-start | bytes 34603012
  35.0 5.6 %copy-start.3 = (f32[2,2816]{1,0:T(2,128)S(1)}, f32[2,2816]{1,0:T(2,128)}, u32[]{:S(2)}) copy-start(f32[2,2816]{1,0:T(2,128)} %param.14) | copy-start | bytes 67588
  35.0 5.6 %copy-start.4 = (f32[2,2816]{1,0:T(2,128)S(1)}, f32[2,2816]{1,0:T(2,128)}, u32[]{:S(2)}) copy-start(f32[2,2816]{1,0:T(2,128)} %param.13) | copy-start | bytes 67588
  37.1 110.1 %all-reduce.3.cloned.1.call-start = ((), (), s32[]{:S(2)}) async-start(), calls=%async_computation.6 | async-start | bytes 524288 | tf_op jit(solution)/shard_map/psum | solution.py:43
  37.3 5.1 %collective-permute-start = (f32[128]{0:T(128)S(1)}, f32[128]{0:T(128)S(1)}, u32[]{:S(2)}, u32[]{:S(2)}) collective-permute-start(f32[128]{0:T(128)S(1)} %fusion.14), channel_id=1, source_target_pairs={{0,4},{4,0},{8,12},{12,8},{1,5},{5,1},{9,13},{13,9},{2,6},{6,2},{1... | collective-permute-start | bytes 1544 | tf_op jit(solution)/shard_map/ppermute | solution.py:27
  42.4 15.6 %collective-permute-start.1 = (f32[128]{0:T(128)S(1)}, f32[128]{0:T(128)S(1)}, u32[]{:S(2)}, u32[]{:S(2)}) collective-permute-start(f32[128]{0:T(128)S(1)} %add.55), channel_id=1, source_target_pairs={{0,8},{4,12},{8,0},{12,4},{1,9},{5,13},{9,1},{13,5},{2,10},{6,14},... | collective-permute-start | bytes 1544 | tf_op jit(solution)/shard_map/ppermute | solution.py:27
  58.0 57.8 %copy-start.5 = (f32[2,1024]{1,0:T(2,128)S(1)}, f32[2,1024]{1,0:T(2,128)}, u32[]{:S(2)}) copy-start(f32[2,1024]{1,0:T(2,128)} %param.15) | copy-start | bytes 24580
  115.8 70.8 %reduce-scatter.9.cloned.1.call-start = ((), (), s32[]{:S(2)}) async-start(), calls=%async_computation.7 | async-start | bytes 1802240 | tf_op jit(solution)/shard_map/reduce_scatter | solution.py:30
  153.0 67.9 %reduce-scatter.11.cloned.1.call-start = ((), (), s32[]{:S(2)}) async-start(), calls=%async_computation.8 | async-start | bytes 1802240 | tf_op jit(solution)/shard_map/reduce_scatter | solution.py:31
  157.8 130.3 %copy-start.6 = (f32[1024]{0:T(1024)S(1)}, f32[1024]{0:T(1024)}, u32[]{:S(2)}) copy-start(f32[1024]{0:T(1024)} %param.17) | copy-start | bytes 12292
  157.8 117.4 %all-reduce.5.cloned.1.call-start = ((), (), s32[]{:S(2)}) async-start(), calls=%async_computation.9 | async-start | bytes 524288 | tf_op jit(solution)/shard_map/psum | solution.py:43
  157.8 3.6 %collective-permute-start.2 = (f32[128]{0:T(128)S(1)}, f32[128]{0:T(128)S(1)}, u32[]{:S(2)}, u32[]{:S(2)}) collective-permute-start(f32[128]{0:T(128)S(1)} %get-tuple-element.9), channel_id=1, source_target_pairs={{0,4},{4,0},{8,12},{12,8},{1,5},{5,1},{9,13},{13,9},{2,6},{6,2},{1... | collective-permute-start | bytes 1544 | tf_op jit(solution)/shard_map/ppermute | solution.py:27
  161.5 4.7 %collective-permute-start.3 = (f32[128]{0:T(128)S(1)}, f32[128]{0:T(128)S(1)}, u32[]{:S(2)}, u32[]{:S(2)}) collective-permute-start(f32[128]{0:T(128)S(1)} %add.61), channel_id=1, source_target_pairs={{0,8},{4,12},{8,0},{12,4},{1,9},{5,13},{9,1},{13,5},{2,10},{6,14},... | collective-permute-start | bytes 1544 | tf_op jit(solution)/shard_map/ppermute | solution.py:27
Sparse Core Ops, SparseCore 0:
  22.3 36.1 reduce-scatter.4
  60.8 32.1 reduce-scatter.6
  115.9 31.2 all-reduce.2
  153.1 33.4 reduce-scatter.8
  188.8 32.1 reduce-scatter.10
  243.8 31.3 all-reduce.4
